TPU v7x, 32 devices: a whole 2x2x4 slice. The times are simulated.
32 devices in a mesh: sp: 4 (over z), fs: 4 (over y, x), tp: 2 (over core).
Axes of the slice: x: 2, y: 2, z: 4, core: 2. Of those that a mesh axis runs over, the one named last changes fastest.
Arguments:
- tokens: bfloat16 [2048, 2048], P(('fs', 'sp'), 'tp'), parts along dimension 0, may hold values from -6 to 6
- norm_gain: float32 [2048], replicated, may hold values from 0.1 to 1.9
- w_recur_in: bfloat16 [2048, 1024], P(None, 'tp'), may hold values from -0.125 to 0.125
- conv_weight: float32 [4, 1024], P(None, 'tp'), may hold values from -3 to 3
- w_gate_decay: bfloat16 [16, 64, 64], P('tp'), may hold values from -0.75 to 0.75
- w_gate_input: bfloat16 [16, 64, 64], P('tp'), may hold values from -0.75 to 0.75
- decay_base: float32 [1024], P('tp'), may hold values from 0 to 0.01, as said below
- extra_decay: float32 [2048, 16], P(('fs', 'sp'), 'tp'), parts along dimension 0, may hold values from 0 to 1, as said below
- w_query: bfloat16 [2048, 1024], P(None, 'tp'), may hold values from -1 to 1
- w_key: bfloat16 [2048, 256], P(None, 'tp'), may hold values from -20 to 20
- w_value: bfloat16 [2048, 256], P(None, 'tp'), may hold values from -0.125 to 0.125
- mix_lambda: float32 [8], P('tp'), may hold values from 0.3 to 0.8
- head_gain: float32 [128], replicated, may hold values from 0.1 to 1.9
- w_out_recur: bfloat16 [1024, 2048], P('tp'), may hold values from -0.125 to 0.125
- w_out_attend: bfloat16 [1024, 2048], P('tp'), may hold values from -0.125 to 0.125
- out_gain: float32 [2048], replicated, may hold values from 0.1 to 1.9
Outputs:
- mixed: bfloat16 [2048, 2048], P(('fs', 'sp', 'tp')), parts along dimension 0
There are 4 independent parts, one for each index of `fs`. A program takes and returns all parts, laid end to end along the dimension named above; an argument that names none is the same for every part. Nothing has to cross between parts.
Inputs may be any that keep to these rules, and one draw needn't show every extreme that they name: `decay_base`: positive rates of each channel. `extra_decay`: non-negative added log-decays.
All inputs are finite; a program needn't handle non-finite values.
Results may differ from a plain program's by a relative error of at most 0.012.
The roundings to bfloat16 on the way count: a program that leaves them out, or rounds other values in their place, can miss the bound.
Values may be sent and summed in bfloat16 or wider, within the bound.
A program may use at most 128 MiB of HBM per device.

v0:
```python
import jax
import jax.numpy as jnp
from jax import lax
from jax.sharding import PartitionSpec as P

D = 2048
HEAD = 64
DV = 128
lru_rate = 8.0
norm_eps = 1e-06


def shifted(block, axis, distance):
    devices = range(lax.axis_size(axis))
    route = [(i - distance, i) for i in devices if i - distance in devices]
    return lax.ppermute(block, axis, route)


def prefix(part, axis, combine, identity):
    place = lax.axis_index(axis)
    gathered = jax.tree.map(lambda a: lax.all_gather(a, axis), part)
    state = jax.tree.map(lambda a, e: jnp.zeros_like(a) + jnp.asarray(e, a.dtype), part, identity)

    def one(lap, state):
        return combine(
            state, jax.tree.map(lambda a: lax.dynamic_index_in_dim(a, lap, 0, False), gathered)
        )

    return lax.fori_loop(0, place, one, state)


def chain(earlier, later):
    return (earlier[0] * later[0], later[0] * earlier[1] + later[1])


def body(
    tokens,
    norm_gain,
    w_recur_in,
    conv_weight,
    w_gate_decay,
    w_gate_input,
    decay_base,
    extra_decay,
    w_query,
    w_key,
    w_value,
    mix_lambda,
    head_gain,
    w_out_recur,
    w_out_attend,
    out_gain,
):
    row_count = tokens.shape[0]
    recur_cols = w_recur_in.shape[1]
    query_cols = w_query.shape[1]
    key_cols = w_key.shape[1]
    all_weights = jnp.concatenate([w_recur_in, w_query, w_key, w_value], axis=1)
    wide_piece = lax.all_gather(tokens, "tp", axis=1, tiled=True).astype(jnp.float32)
    scaled = (wide_piece * norm_gain).astype(jnp.bfloat16)
    accum = jnp.dot(scaled, all_weights, preferred_element_type=jnp.float32)
    squares = jnp.sum(wide_piece * wide_piece, axis=1, keepdims=True)
    accum, squares = (accum, squares)
    inverse = lax.rsqrt(squares / D + norm_eps)
    projected = (accum * inverse).astype(jnp.bfloat16)
    recur_in = projected[:, :recur_cols]
    queries = projected[:, recur_cols : recur_cols + query_cols]
    keys = projected[:, recur_cols + query_cols : recur_cols + query_cols + key_cols]
    values = projected[:, recur_cols + query_cols + key_cols :]
    taps = conv_weight.shape[0]
    carried_rows = shifted(recur_in[row_count - (taps - 1) :], "sp", 1)
    padded = jnp.concatenate([carried_rows, recur_in], axis=0).astype(jnp.float32)
    conv_acc = jnp.zeros((row_count, recur_cols), jnp.float32)
    for offset in range(taps):
        conv_acc = conv_acc + conv_weight[offset] * padded[offset : offset + row_count]
    conv_in = conv_acc.astype(jnp.bfloat16)
    gate_blocks = w_gate_decay.shape[0]
    blocks = conv_in.reshape(row_count, gate_blocks, HEAD)
    decay_gate = jax.nn.sigmoid(
        jnp.einsum("thi,hij->thj", blocks, w_gate_decay, preferred_element_type=jnp.float32)
    ).reshape(row_count, recur_cols)
    input_gate = jax.nn.sigmoid(
        jnp.einsum("thi,hij->thj", blocks, w_gate_input, preferred_element_type=jnp.float32)
    ).reshape(row_count, recur_cols)
    log_decay = -lru_rate * decay_gate * decay_base - jnp.repeat(extra_decay, HEAD, axis=1)
    decay = jnp.exp(log_decay)
    inject = jnp.sqrt(-jnp.expm1(2.0 * log_decay)) * input_gate * conv_in.astype(jnp.float32)
    decay_cum, local_state = lax.associative_scan(chain, (decay, inject), axis=0)
    identity = (jnp.ones((recur_cols,), jnp.float32), jnp.zeros((recur_cols,), jnp.float32))
    carried = prefix((decay_cum[row_count - 1], local_state[row_count - 1]), "sp", chain, identity)
    recur_out = (local_state + decay_cum * carried[1]).astype(jnp.bfloat16)
    kv_local = key_cols // (2 * HEAD)
    heads_local = query_cols // (2 * HEAD)
    group_size = heads_local // kv_local
    local_query = queries.reshape(row_count, kv_local, group_size, 2, HEAD)
    offset_rows = lax.axis_index("sp") * row_count
    positions = offset_rows + jnp.arange(row_count, dtype=jnp.int32)
    last_position = offset_rows + row_count - 1
    lambdas = mix_lambda.reshape(kv_local, group_size)
    start_state = (
        jnp.full((2, kv_local, group_size, row_count), -1e30, jnp.float32),
        jnp.zeros((2, kv_local, group_size, row_count), jnp.float32),
        jnp.zeros((2, row_count, kv_local, group_size, DV), jnp.float32),
    )
    key_piece = lax.all_gather(keys, "sp", axis=0, tiled=True)
    value_piece = lax.all_gather(values, "sp", axis=0, tiled=True)
    count = key_piece.shape[0]

    def update(state):
        peaks, totals, attends = state
        key_three = key_piece.reshape(count, kv_local, 2, HEAD)
        value_three = value_piece.reshape(count, kv_local, DV)
        allowed = positions[:, None] >= jnp.arange(count, dtype=jnp.int32)[None, :]
        new_peaks, new_totals, new_attends = ([], [], [])
        for mapping in range(2):
            scores = jnp.einsum(
                "bkgd,tkd->kgbt",
                local_query[:, :, :, mapping, :],
                key_three[:, :, mapping, :],
                preferred_element_type=jnp.float32,
            ) * HEAD ** (-0.5)
            scores = jnp.where(allowed, scores, -jnp.inf)
            peak = jnp.maximum(peaks[mapping], jnp.max(scores, axis=-1))
            correction = jnp.exp(peaks[mapping] - peak)
            expo = jnp.exp(scores - peak[..., None])
            new_totals.append(totals[mapping] * correction + jnp.sum(expo, axis=-1))
            gained = jnp.einsum(
                "kgbt,tke->bkge",
                expo.astype(jnp.bfloat16),
                value_three,
                preferred_element_type=jnp.float32,
            )
            new_attends.append(
                attends[mapping] * jnp.transpose(correction, (2, 0, 1))[..., None] + gained
            )
            new_peaks.append(peak)
        return (jnp.stack(new_peaks), jnp.stack(new_totals), jnp.stack(new_attends))

    peaks, totals, attends = lax.cond(
        jnp.int32(0) <= last_position, update, lambda state: state, start_state
    )
    first = attends[0] / jnp.transpose(totals[0], (2, 0, 1))[..., None]
    second = attends[1] / jnp.transpose(totals[1], (2, 0, 1))[..., None]
    head_out = (first - lambdas[None, :, :, None] * second).reshape(row_count, heads_local, DV)
    normed = (
        head_out
        * lax.rsqrt(jnp.mean(head_out * head_out, axis=-1, keepdims=True) + norm_eps)
        * head_gain
    )
    attend_out = normed.astype(jnp.bfloat16).reshape(row_count, heads_local * DV)
    recur_rows, attend_rows = (
        lax.all_to_all(recur_out, "tp", split_axis=0, concat_axis=1, tiled=True),
        lax.all_to_all(attend_out, "tp", split_axis=0, concat_axis=1, tiled=True),
    )
    whole_recur, whole_attend = (
        lax.all_gather(w_out_recur, "tp", axis=0, tiled=True),
        lax.all_gather(w_out_attend, "tp", axis=0, tiled=True),
    )
    merged = jnp.dot(recur_rows, whole_recur, preferred_element_type=jnp.float32) + jnp.dot(
        attend_rows, whole_attend, preferred_element_type=jnp.float32
    )
    final = (
        merged * lax.rsqrt(jnp.mean(merged * merged, axis=1, keepdims=True) + norm_eps) * out_gain
    )
    return final.astype(jnp.bfloat16)


def solution(mesh):
    in_specs = (
        P(("fs", "sp"), "tp"),
        P(),
        P(None, "tp"),
        P(None, "tp"),
        P("tp", None, None),
        P("tp", None, None),
        P("tp"),
        P(("fs", "sp"), "tp"),
        P(None, "tp"),
        P(None, "tp"),
        P(None, "tp"),
        P("tp"),
        P(),
        P("tp", None),
        P("tp", None),
        P(),
    )
    out_specs = P(("fs", "sp", "tp"), None)
    return jax.shard_map(body, mesh=mesh, in_specs=in_specs, out_specs=out_specs, check_vma=False)
```

profile of v0, /device:TPU:0, one launch (start us, length us, event | category | flops | bytes accessed | tf_op | source)
XLA Modules:
  0.0 101.6 jit_solution(12139623973826426824)
XLA Ops:
  6.5 0.7 all-gather.5.cloned.1.call-update
  7.3 2.5 %all_gather.21 = bf16[128,2048]{1,0:T(8,128)(2,1)S(1)} all-gather(bf16[128,1024]{1,0:T(8,128)(2,1)} %param.20), channel_id=1, replica_groups=mesh['sp'=4,'fs'=4,'tp'=2] {'tp'}, dimensions={1}, use_global_device_ids=true | all-gather | bytes 786432 | tf_op jit(solution)/shard_map/all_gather | solution.py:59
  9.8 0.2 fusion.43
  10.0 3.2 %fusion.33 = bf16[128,1280]{1,0:T(8,128)(2,1)S(1)} fusion(bf16[2048,128]{1,0:T(8,128)(2,1)} %param.30, bf16[2048,128]{1,0:T(8,128)(2,1)} %param.29, bf16[2048,512]{1,0:T(8,128)(2,1)} %param.28, bf16[2048,512]{1,0:T(8,128)(2,1)} %param.22, bf16[128,2048]{1,0:T(8,128)(2,1)S(1)} %all_gather.21, f32[2048]{0:T(1024)} %param.21, f32[128]{0:T(128)S(1)} %add_rsqrt_fusion.2), kind=kOutput, calls=%fused_computation.52 | convolution fusion | flops 693174272 | bytes 6103552 | tf_op jit(solution)/shard_map/dot_general | solution.py:61
  13.2 4.8 %collective-permute-start = (bf16[3,512]{1,0:T(4,128)(2,1)S(1)}, bf16[3,512]{1,0:T(4,128)(2,1)S(1)}, u32[]{:S(2)}, u32[]{:S(2)}) collective-permute-start(bf16[3,512]{1,0:T(4,128)(2,1)S(1)} %slice.358), channel_id=1, source_target_pairs={{0,8},{8,16},{16,24},{1,9},{9,17},{17,25},{2,10},{10,18},{18,26},{... | collective-permute-start | bytes 9224 | tf_op jit(solution)/shard_map/ppermute | solution.py:16
  18.0 13.6 %all_gather.25 = bf16[512,128]{1,0:T(8,128)(2,1)S(1)} all-gather(bf16[128,128]{1,0:T(8,128)(2,1)S(1)} %get-tuple-element.115), channel_id=1, replica_groups=mesh['sp'=4,'fs'=4,'tp'=2] {'sp'}, dimensions={0}, use_global_device_ids=true | all-gather | bytes 163840 | tf_op jit(solution)/shard_map/all_gather | solution.py:105
  31.6 13.4 %all_gather.26 = bf16[512,128]{1,0:T(8,128)(2,1)S(1)} all-gather(bf16[128,128]{1,0:T(8,128)(2,1)S(1)} %get-tuple-element.114), channel_id=1, replica_groups=mesh['sp'=4,'fs'=4,'tp'=2] {'sp'}, dimensions={0}, use_global_device_ids=true | all-gather | bytes 163840 | tf_op jit(solution)/shard_map/all_gather | solution.py:106
  45.0 2.2 %conditional.1 = (f32[2,1,4,128]{3,2,1,0:T(4,128)S(1)}, f32[2,128,1,4,128]{4,1,3,2,0:T(8,128)S(1)}) conditional(s32[]{:T(128)} %convert_element_type.45, () %tuple.21, (s32[]{:T(128)}, s32[128]{0:T(128)S(1)}, bf16[512,128]{1,0:T(8,128)(2,1)S(1)}, bf16[128,1280]{1,0:T(8,128)(2,1)S(1)}, bf16[512,128]{1,0:T(8,128)(2,1)S(1)}) %tuple.22), branch_computations={%region_3.4_spmd, %region_4.9_spmd} | conditional | flops 205328512 | bytes 9819668 | solution.py:139
  45.0 0.2 copy.57
  45.3 0.1 copy.56
  45.4 0.3 fusion.65
  45.8 0.2 fusion.11
  46.0 0.3 fusion.66
  46.3 0.2 fusion.9
  46.5 0.4 fusion.5
  46.9 0.4 fusion.7
  47.3 0.0 copy-start.6
  47.3 0.1 copy.72
  47.4 0.1 copy.73
  47.5 0.3 fusion.53
  47.9 0.1 copy.62
  48.0 0.2 mul.337
  48.2 0.1 mul.338
  48.3 0.0 copy-start.2
  48.3 0.0 copy-start.5
  48.4 0.2 copy.58
  48.6 0.1 squeeze.135
  48.7 0.2 copy.60
  48.9 0.1 squeeze.137
  49.0 0.2 div.75.clone
  49.2 0.1 div.76
  49.3 0.2 div.79.clone
  49.5 0.1 div.80
  49.6 0.1 broadcast_bitcast_fusion
  49.7 0.8 multiply_convert_fusion.1
  50.5 3.4 %all-to-all-start.1 = ((bf16[2,64,512]{2,1,0:T(8,128)(2,1)}), bf16[2,64,512]{2,1,0:T(8,128)(2,1)S(1)}, u32[]{:S(2)}, u32[]{:S(2)}) async-start(bf16[2,64,512]{2,1,0:T(8,128)(2,1)} %multiply_convert_fusion.1), calls=%async_computation.1 | async-start | bytes 262144 | tf_op jit(solution)/shard_map/all_to_all | solution.py:153
  53.8 0.0 all-gather.7.cloned.1.call-start
  53.9 0.7 all-gather.7.cloned.1.call-update
  54.7 0.1 copy.52
  54.8 0.5 all-to-all-done.1
  55.4 0.1 fusion.47
  55.5 0.1 copy.49
  55.6 0.3 fusion.41
  55.9 0.1 copy.51
  56.0 0.3 fusion.38
  56.3 0.1 copy.54
  56.5 0.3 convert_multiply_fusion.2
  56.8 0.1 slice.284
  56.9 0.1 slice.285
  57.0 0.1 slice.283
  57.1 0.1 slice.287
  58.2 0.2 slice.282
  58.4 0.2 slice.331
  59.5 0.1 fusion.54
  59.6 11.9 %all-gather.1 = f32[4,1,512]{2,1,0:T(1,128)S(1)} all-gather(f32[1,1,512]{2,1,0:T(1,128)S(1)} %add_bitcast_fusion.2), channel_id=1, replica_groups=mesh['sp'=4,'fs'=4,'tp'=2] {'sp'}, dimensions={0}, use_global_device_ids=true | all-gather | bytes 10240 | tf_op jit(solution)/shard_map/all_gather | solution.py:21
  71.7 11.9 %all-gather = f32[4,1,512]{2,1,0:T(1,128)S(1)} all-gather(f32[1,1,512]{2,1,0:T(1,128)S(1)} %add_bitcast_fusion.3), channel_id=1, replica_groups=mesh['sp'=4,'fs'=4,'tp'=2] {'sp'}, dimensions={0}, use_global_device_ids=true | all-gather | bytes 10240 | tf_op jit(solution)/shard_map/all_gather | solution.py:21
  83.6 0.1 add_convert_fusion
  83.8 3.8 %all_to_all.35 = bf16[2,64,512]{2,1,0:T(8,128)(2,1)S(1)} all-to-all(bf16[2,64,512]{2,1,0:T(8,128)(2,1)S(1)} %bitcast.174), channel_id=1, replica_groups=mesh['sp'=4,'fs'=4,'tp'=2] {'tp'}, dimensions={0} | all-to-all | bytes 262144 | tf_op jit(solution)/shard_map/all_to_all | solution.py:152
  87.6 0.0 all-gather.5.cloned.1.call-done
  87.6 0.0 copy-start.1
  87.6 3.0 %fusion.71 = f32[64,2048]{1,0:T(8,128)S(1)} fusion(bf16[64,1024]{1,0:T(8,128)(2,1)S(1)} %bitcast.175, bf16[1024,2048]{1,0:T(8,128)(2,1)} %all-gather.5.cloned.1.call-done), kind=kOutput, calls=%fused_computation.154 | convolution fusion | flops 268435456 | bytes 4849664 | tf_op jit(solution)/shard_map/dot_general | solution.py:159
  90.7 0.0 all-gather.7.cloned.1.call-done
  90.7 3.2 %multiply_reduce_fusion = (f32[64]{0:T(128)S(1)}, f32[64,2048]{1,0:T(8,128)S(1)}) fusion(f32[64,2048]{1,0:T(8,128)S(1)} %fusion.71, bf16[64,1024]{1,0:T(8,128)(2,1)S(1)} %bitcast.173, bf16[1024,2048]{1,0:T(8,128)(2,1)} %all-gather.7.cloned.1.call-done), kind=kOutput, calls=%fused_computation.67 | convolution fusion | flops 268828608 | bytes 5374208 | tf_op jit(solution)/shard_map/dot_general | solution.py:159
  93.9 0.8 multiply_convert_fusion
  (139 shorter events, 1.9 us)
Async XLA Ops:
  6.5 49.1 %copy-start = (bf16[8,64,64]{2,1,0:T(8,128)(2,1)S(1)}, bf16[8,64,64]{2,1,0:T(8,128)(2,1)}, u32[]{:S(2)}) copy-start(bf16[8,64,64]{2,1,0:T(8,128)(2,1)} %param.24) | copy-start | bytes 196612
  6.5 81.1 %all-gather.5.cloned.1.call-start = ((), (), s32[]{:S(2)}) async-start(), calls=%async_computation.2 | async-start | bytes 6291456 | tf_op jit(solution)/shard_map/all_gather | solution.py:156
  13.2 42.1 %collective-permute-start = (bf16[3,512]{1,0:T(4,128)(2,1)S(1)}, bf16[3,512]{1,0:T(4,128)(2,1)S(1)}, u32[]{:S(2)}, u32[]{:S(2)}) collective-permute-start(bf16[3,512]{1,0:T(4,128)(2,1)S(1)} %slice.358), channel_id=1, source_target_pairs={{0,8},{8,16},{16,24},{1,9},{9,17},{17,25},{2,10},{10,18},{18,26},{... | collective-permute-start | bytes 9224 | tf_op jit(solution)/shard_map/ppermute | solution.py:16
  45.0 2.5 %copy-start.4 = (f32[4]{0:T(128)S(1)}, f32[4]{0:T(128)}, u32[]{:S(2)}) copy-start(f32[4]{0:T(128)} %param.31) | copy-start | bytes 52
  47.3 2.3 %copy-start.6 = (f32[128]{0:T(128)S(1)}, f32[128]{0:T(128)}, u32[]{:S(2)}) copy-start(f32[128]{0:T(128)} %param.32) | copy-start | bytes 1540
  48.3 6.3 %copy-start.2 = (f32[4,512]{1,0:T(4,128)S(1)}, f32[4,512]{1,0:T(4,128)}, u32[]{:S(2)}) copy-start(f32[4,512]{1,0:T(4,128)} %param.23) | copy-start | bytes 24580
  48.3 6.3 %copy-start.5 = (f32[512]{0:T(512)S(1)}, f32[512]{0:T(512)}, u32[]{:S(2)}) copy-start(f32[512]{0:T(512)} %param.26) | copy-start | bytes 6148
  48.4 6.3 %copy-start.3 = (f32[128,8]{0,1:T(8,128)S(1)}, f32[128,8]{0,1:T(8,128)}, u32[]{:S(2)}) copy-start(f32[128,8]{0,1:T(8,128)} %param.27) | copy-start | bytes 12292
  49.7 6.4 %copy-start.7 = (bf16[8,64,64]{2,1,0:T(8,128)(2,1)S(1)}, bf16[8,64,64]{2,1,0:T(8,128)(2,1)}, u32[]{:S(2)}) copy-start(bf16[8,64,64]{2,1,0:T(8,128)(2,1)} %param.25) | copy-start | bytes 196612
  50.5 4.8 %all-to-all-start.1 = ((bf16[2,64,512]{2,1,0:T(8,128)(2,1)}), bf16[2,64,512]{2,1,0:T(8,128)(2,1)S(1)}, u32[]{:S(2)}, u32[]{:S(2)}) async-start(bf16[2,64,512]{2,1,0:T(8,128)(2,1)} %multiply_convert_fusion.1), calls=%async_computation.1 | async-start | bytes 262144 | tf_op jit(solution)/shard_map/all_to_all | solution.py:153
  53.8 36.9 %all-gather.7.cloned.1.call-start = ((), (), s32[]{:S(2)}) async-start(), calls=%async_computation.3 | async-start | bytes 6291456 | tf_op jit(solution)/shard_map/all_gather | solution.py:157
  87.6 6.3 %copy-start.1 = (f32[2048]{0:T(1024)S(1)}, f32[2048]{0:T(1024)}, u32[]{:S(2)}) copy-start(f32[2048]{0:T(1024)} %param.35) | copy-start | bytes 24580
Sparse Core Ops, SparseCore 0:
  8.9 16.3 all-gather.4
  56.2 12.8 all-gather.6
where the time goes:
time: 102 us
  blocking collectives  57.2 us (56%)
  between operations  14.4 us (14%)
  matrix products  11.3 us (11%)
  starting transfers between devices  8.26 us (8%)
  local copies, waits for them, and re-layouts  4.75 us (5%)
  other arithmetic  3.69 us (4%)
  waiting for transfers between devices  1.91 us (2%)
    all_gather x2, blocking collectives, prefix(): gathered = jax.tree.map(lambda a: lax.all_gather(a, axis), part)  23.9 us
    all_gather x1, blocking collectives, body(): key_piece = lax.all_gather(keys, 'sp', axis=0, tiled=True)  13.6 us
    all_gather x1, blocking collectives, body(): value_piece = lax.all_gather(values, 'sp', axis=0, tiled=True)  13.4 us
    ppermute x1, starting transfers between devices, shifted(): return lax.ppermute(block, axis, route)  4.84 us
    all_to_all x1, blocking collectives, body(): lax.all_to_all(recur_out, 'tp', split_axis=0, concat_axis=1, tiled=True)  3.84 us
    all_to_all x1, starting transfers between devices, body(): lax.all_to_all(attend_out, 'tp', split_axis=0, concat_axis=1, tiled=True)  3.38 us
    dot_general x1, matrix products, body(): accum = jnp.dot(scaled, all_weights, preferred_element_type=jnp.float32)  3.19 us
    dot_general x1, matrix products, body(): jnp.dot(attend_rows, whole_attend, preferred_element_type=jnp.float32)  3.16 us
  transfers between devices with their start and end apart: 4, of which 1 were waited for; matrix products, arithmetic and copies ran while one was open for 15% of the time, Pallas kernels for 0%

commit v1 on v0

--- a/solution.py
+++ b/solution.py
@@ -102,7 +102,12 @@
         jnp.zeros((2, kv_local, group_size, row_count), jnp.float32),
         jnp.zeros((2, row_count, kv_local, group_size, DV), jnp.float32),
     )
-    key_piece = lax.all_gather(keys, "sp", axis=0, tiled=True)
+    ring = [keys]
+    for hop in range(3):
+        ring.append(lax.ppermute(ring[-1], "sp", [(dev, (dev + 1) % 4) for dev in range(4)]))
+    key_piece = jnp.roll(
+        jnp.concatenate(ring[::-1], axis=0), (lax.axis_index("sp") + 1) * ring[0].shape[0], axis=0
+    )
     value_piece = lax.all_gather(values, "sp", axis=0, tiled=True)
     count = key_piece.shape[0]
 

time: 102 us -> 98.2 us (0.963)
  blocking collectives: 57.2 us -> 48.3 us
  waiting for transfers between devices: 1.91 us -> 9.16 us
  starting transfers between devices: 8.26 us -> 6.55 us
    all_gather x1 -> x0, blocking collectives: 13.6 us -> none  [body(): key_piece = lax.all_gather(keys, 'sp', axis=0, tiled=True)]
    ppermute x0 -> x3, waiting for transfers between devices: none -> 7.42 us  [body(): lax.ppermute(ring[-1], 'sp', [(dev, (dev + 1) % 4) for dev in range(4)])]
    all_to_all x0 -> x1, blocking collectives: none -> 3.84 us  [body(): lax.all_to_all(attend_out, 'tp', split_axis=0, concat_axis=1, tiled=True)]
    all_to_all x1 -> x0, starting transfers between devices: 3.38 us -> none  [body(): lax.all_to_all(attend_out, 'tp', split_axis=0, concat_axis=1, tiled=True)]
    ppermute x0 -> x3, starting transfers between devices: none -> 3.04 us  [body(): lax.ppermute(ring[-1], 'sp', [(dev, (dev + 1) % 4) for dev in range(4)])]
    ppermute x1, starting transfers between devices: 4.84 us -> 3.47 us  [shifted(): return lax.ppermute(block, axis, route)]
  transfers between devices with their start and end apart: 4 -> 6, of which waited for: 1 -> 3; matrix products, arithmetic and copies ran while one was open for 15% -> 16% of each run, Pallas kernels for 0% -> 0%
where the time goes in v1:
time: 98.2 us; the launch traced here: 97.9 us
  blocking collectives  48.3 us (49%)
  between operations  14.4 us (15%)
  matrix products  11.3 us (12%)
  waiting for transfers between devices  9.16 us (9%)
  starting transfers between devices  6.55 us (7%)
  local copies, waits for them, and re-layouts  4.98 us (5%)
  other arithmetic  3.04 us (3%)
    all_gather x2, blocking collectives, prefix(): gathered = jax.tree.map(lambda a: lax.all_gather(a, axis), part)  24.8 us
    all_gather x1, blocking collectives, body(): value_piece = lax.all_gather(values, 'sp', axis=0, tiled=True)  13.3 us
    ppermute x3, waiting for transfers between devices, body(): lax.ppermute(ring[-1], 'sp', [(dev, (dev + 1) % 4) for dev in range(4)])  7.42 us
    all_to_all x1, blocking collectives, body(): lax.all_to_all(recur_out, 'tp', split_axis=0, concat_axis=1, tiled=True)  3.84 us
    all_to_all x1, blocking collectives, body(): lax.all_to_all(attend_out, 'tp', split_axis=0, concat_axis=1, tiled=True)  3.84 us
    ppermute x1, starting transfers between devices, shifted(): return lax.ppermute(block, axis, route)  3.47 us
    dot_general x1, matrix products, body(): accum = jnp.dot(scaled, all_weights, preferred_element_type=jnp.float32)  3.19 us
    dot_general x1, matrix products, body(): jnp.dot(attend_rows, whole_attend, preferred_element_type=jnp.float32)  3.16 us
  transfers between devices with their start and end apart: 6, of which 3 were waited for; matrix products, arithmetic and copies ran while one was open for 16% of the time, Pallas kernels for 0%

profile of v1, /device:TPU:0, one launch (start us, length us, event | category | flops | bytes accessed | tf_op | source)
XLA Modules:
  0.0 97.9 jit_solution(6308331883714014534)
XLA Ops:
  6.5 0.7 all-gather.5.cloned.1.call-update
  7.3 0.0 all-gather.7.cloned.1.call-start
  7.3 2.5 %all_gather.18 = bf16[128,2048]{1,0:T(8,128)(2,1)S(1)} all-gather(bf16[128,1024]{1,0:T(8,128)(2,1)} %param.20), channel_id=1, replica_groups=mesh['sp'=4,'fs'=4,'tp'=2] {'tp'}, dimensions={1}, use_global_device_ids=true | all-gather | bytes 786432 | tf_op jit(solution)/shard_map/all_gather | solution.py:59
  9.8 0.2 fusion.43
  10.1 3.2 %fusion.33 = bf16[128,1280]{1,0:T(8,128)(2,1)S(1)} fusion(bf16[2048,128]{1,0:T(8,128)(2,1)} %param.30, bf16[2048,128]{1,0:T(8,128)(2,1)} %param.29, bf16[2048,512]{1,0:T(8,128)(2,1)} %param.28, bf16[2048,512]{1,0:T(8,128)(2,1)} %param.22, bf16[128,2048]{1,0:T(8,128)(2,1)S(1)} %all_gather.18, f32[2048]{0:T(1024)} %param.21, f32[128]{0:T(128)S(1)} %add_rsqrt_fusion.2), kind=kOutput, calls=%fused_computation.53 | convolution fusion | flops 693174272 | bytes 6103552 | tf_op jit(solution)/shard_map/dot_general | solution.py:61
  13.3 3.0 %collective-permute-start.1 = (bf16[128,128]{1,0:T(8,128)(2,1)S(1)}, bf16[128,128]{1,0:T(8,128)(2,1)S(1)}, u32[]{:S(2)}, u32[]{:S(2)}) collective-permute-start(bf16[128,128]{1,0:T(8,128)(2,1)S(1)} %slice.430), channel_id=1, source_target_pairs={{0,8},{8,16},{16,24},{24,0},{1,9},{9,17},{17,25},{25,1},{2,10},{10... | collective-permute-start | bytes 98312 | tf_op jit(solution)/shard_map/ppermute | solution.py:107
  16.3 3.5 %collective-permute-start = (bf16[3,512]{1,0:T(4,128)(2,1)S(1)}, bf16[3,512]{1,0:T(4,128)(2,1)S(1)}, u32[]{:S(2)}, u32[]{:S(2)}) collective-permute-start(bf16[3,512]{1,0:T(4,128)(2,1)S(1)} %slice.378), channel_id=1, source_target_pairs={{0,8},{8,16},{16,24},{1,9},{9,17},{17,25},{2,10},{10,18},{18,26},{... | collective-permute-start | bytes 9224 | tf_op jit(solution)/shard_map/ppermute | solution.py:16
  19.8 0.0 all-gather.7.cloned.1.call-update
  19.8 0.1 broadcast_bitcast_fusion
  20.0 0.1 copy.52
  20.1 1.0 collective-permute-done
  21.1 0.1 fusion.47
  21.2 0.1 copy.49
  21.4 0.3 fusion.41
  21.7 0.1 copy.51
  21.8 0.3 fusion.38
  22.1 0.1 copy.54
  22.2 0.3 convert_multiply_fusion.2
  22.6 0.1 slice.299
  22.7 0.1 slice.300
  22.8 0.1 slice.298
  22.9 0.1 slice.302
  23.9 0.2 slice.297
  24.1 0.2 slice.346
  25.2 0.1 fusion.54
  25.5 12.9 %all-gather.1 = f32[4,1,512]{2,1,0:T(1,128)S(1)} all-gather(f32[1,1,512]{2,1,0:T(1,128)S(1)} %add_bitcast_fusion.2), channel_id=1, replica_groups=mesh['sp'=4,'fs'=4,'tp'=2] {'sp'}, dimensions={0}, use_global_device_ids=true | all-gather | bytes 10240 | tf_op jit(solution)/shard_map/all_gather | solution.py:21
  38.4 11.9 %all-gather = f32[4,1,512]{2,1,0:T(1,128)S(1)} all-gather(f32[1,1,512]{2,1,0:T(1,128)S(1)} %add_bitcast_fusion.3), channel_id=1, replica_groups=mesh['sp'=4,'fs'=4,'tp'=2] {'sp'}, dimensions={0}, use_global_device_ids=true | all-gather | bytes 10240 | tf_op jit(solution)/shard_map/all_gather | solution.py:21
  50.3 0.1 collective-permute-start.2
  50.4 5.7 %collective-permute-done.2 = bf16[128,128]{1,0:T(8,128)(2,1)S(1)} collective-permute-done((bf16[128,128]{1,0:T(8,128)(2,1)S(1)}, bf16[128,128]{1,0:T(8,128)(2,1)S(1)}, u32[]{:S(2)}, u32[]{:S(2)}) %collective-permute-start.2) | collective-permute-done | bytes 32800 | tf_op jit(solution)/shard_map/ppermute | solution.py:107
  56.1 0.1 add_convert_fusion
  56.2 3.8 %all_to_all.35 = bf16[2,64,512]{2,1,0:T(8,128)(2,1)S(1)} all-to-all(bf16[2,64,512]{2,1,0:T(8,128)(2,1)S(1)} %bitcast.175), channel_id=1, replica_groups=mesh['sp'=4,'fs'=4,'tp'=2] {'tp'}, dimensions={0} | all-to-all | bytes 262144 | tf_op jit(solution)/shard_map/all_to_all | solution.py:157
  60.0 1.7 %collective-permute-done.3 = bf16[128,128]{1,0:T(8,128)(2,1)S(1)} collective-permute-done((bf16[128,128]{1,0:T(8,128)(2,1)S(1)}, bf16[128,128]{1,0:T(8,128)(2,1)S(1)}, u32[]{:S(2)}, u32[]{:S(2)}) %collective-permute-start.3) | collective-permute-done | bytes 32800 | tf_op jit(solution)/shard_map/ppermute | solution.py:107
  61.9 13.3 %all_gather.22 = bf16[512,128]{1,0:T(8,128)(2,1)S(1)} all-gather(bf16[128,128]{1,0:T(8,128)(2,1)S(1)} %get-tuple-element.245), channel_id=1, replica_groups=mesh['sp'=4,'fs'=4,'tp'=2] {'sp'}, dimensions={0}, use_global_device_ids=true | all-gather | bytes 163840 | tf_op jit(solution)/shard_map/all_gather | solution.py:111
  75.2 2.4 %conditional.1 = (f32[2,1,4,128]{3,2,1,0:T(4,128)S(1)}, f32[2,128,1,4,128]{4,1,3,2,0:T(8,128)S(1)}) conditional(s32[]{:T(128)} %convert_element_type.51, () %tuple.32, (s32[]{:T(128)}, s32[128]{0:T(128)S(1)}, s32[]{:T(128)}, s32[]{:T(128)}, bf16[1024,128]{1,0:T(8,128)(2,1)S(1)}, /*index=5*/bf16[128,1280]{1,0:T(8,128)(2,1)S(1)}, ...), branch_computations={%region_3.4_spmd, %region_4.9_spmd.clone} | conditional | flops 205328528 | bytes 10344115 | solution.py:144
  75.2 0.1 copy.56
  75.4 0.1 constant_dynamic-slice_fusion.2
  75.5 0.2 copy.57
  75.8 0.3 fusion.65
  76.2 0.2 fusion.11
  76.3 0.3 fusion.66
  76.7 0.2 fusion.9
  76.9 0.4 fusion.5
  77.2 0.4 fusion.7
  77.7 0.1 copy.72
  77.8 0.1 copy.73
  77.9 0.3 fusion.53
  78.2 0.1 copy.62
  78.3 0.2 mul.347
  78.5 0.1 mul.348
  78.7 0.2 copy.58
  78.9 0.1 squeeze.165
  79.0 0.2 copy.60
  79.2 0.1 squeeze.167
  79.3 0.2 div.75.clone
  79.5 0.1 div.76
  79.6 0.2 div.79.clone
  79.8 0.1 div.80
  79.9 0.1 multiply_convert_fusion.1
  80.1 3.8 %all_to_all.36 = bf16[2,64,512]{2,1,0:T(8,128)(2,1)S(1)} all-to-all(bf16[2,64,512]{2,1,0:T(8,128)(2,1)S(1)} %multiply_convert_fusion.1), channel_id=1, replica_groups=mesh['sp'=4,'fs'=4,'tp'=2] {'tp'}, dimensions={0} | all-to-all | bytes 262144 | tf_op jit(solution)/shard_map/all_to_all | solution.py:158
  83.9 0.0 all-gather.5.cloned.1.call-done
  84.0 3.0 %fusion.71 = f32[64,2048]{1,0:T(8,128)S(1)} fusion(bf16[64,1024]{1,0:T(8,128)(2,1)S(1)} %bitcast.173, bf16[1024,2048]{1,0:T(8,128)(2,1)} %all-gather.5.cloned.1.call-done), kind=kOutput, calls=%fused_computation.163 | convolution fusion | flops 268435456 | bytes 4849664 | tf_op jit(solution)/shard_map/dot_general | solution.py:164
  87.0 0.0 all-gather.7.cloned.1.call-done
  87.0 3.2 %multiply_reduce_fusion = (f32[64]{0:T(128)S(1)}, f32[64,2048]{1,0:T(8,128)S(1)}) fusion(f32[64,2048]{1,0:T(8,128)S(1)} %fusion.71, bf16[64,1024]{1,0:T(8,128)(2,1)S(1)} %bitcast.174, bf16[1024,2048]{1,0:T(8,128)(2,1)} %all-gather.7.cloned.1.call-done), kind=kOutput, calls=%fused_computation.68 | convolution fusion | flops 268828608 | bytes 5374208 | tf_op jit(solution)/shard_map/dot_general | solution.py:164
  90.2 0.8 multiply_convert_fusion
  (152 shorter events, 2.0 us)
Async XLA Ops:
  6.5 14.8 %copy-start = (bf16[8,64,64]{2,1,0:T(8,128)(2,1)S(1)}, bf16[8,64,64]{2,1,0:T(8,128)(2,1)}, u32[]{:S(2)}) copy-start(bf16[8,64,64]{2,1,0:T(8,128)(2,1)} %param.24) | copy-start | bytes 196612
  6.5 77.4 %all-gather.5.cloned.1.call-start = ((), (), s32[]{:S(2)}) async-start(), calls=%async_computation.2 | async-start | bytes 6291456 | tf_op jit(solution)/shard_map/all_gather | solution.py:161
  7.3 79.8 %all-gather.7.cloned.1.call-start = ((), (), s32[]{:S(2)}) async-start(), calls=%async_computation.3 | async-start | bytes 6291456 | tf_op jit(solution)/shard_map/all_gather | solution.py:162
  10.0 9.8 %copy-start.2 = (f32[4,512]{1,0:T(4,128)S(1)}, f32[4,512]{1,0:T(4,128)}, u32[]{:S(2)}) copy-start(f32[4,512]{1,0:T(4,128)} %param.23) | copy-start | bytes 24580
  10.0 9.8 %copy-start.4 = (f32[4]{0:T(128)S(1)}, f32[4]{0:T(128)}, u32[]{:S(2)}) copy-start(f32[4]{0:T(128)} %param.31) | copy-start | bytes 52
  10.0 9.8 %copy-start.6 = (f32[128]{0:T(128)S(1)}, f32[128]{0:T(128)}, u32[]{:S(2)}) copy-start(f32[128]{0:T(128)} %param.32) | copy-start | bytes 1540
  10.0 9.9 %copy-start.5 = (f32[512]{0:T(512)S(1)}, f32[512]{0:T(512)}, u32[]{:S(2)}) copy-start(f32[512]{0:T(512)} %param.26) | copy-start | bytes 6148
  10.1 9.9 %copy-start.3 = (f32[128,8]{0,1:T(8,128)S(1)}, f32[128,8]{0,1:T(8,128)}, u32[]{:S(2)}) copy-start(f32[128,8]{0,1:T(8,128)} %param.27) | copy-start | bytes 12292
  13.3 8.5 %copy-start.7 = (bf16[8,64,64]{2,1,0:T(8,128)(2,1)S(1)}, bf16[8,64,64]{2,1,0:T(8,128)(2,1)}, u32[]{:S(2)}) copy-start(bf16[8,64,64]{2,1,0:T(8,128)(2,1)} %param.25) | copy-start | bytes 196612
  13.3 37.0 %collective-permute-start.1 = (bf16[128,128]{1,0:T(8,128)(2,1)S(1)}, bf16[128,128]{1,0:T(8,128)(2,1)S(1)}, u32[]{:S(2)}, u32[]{:S(2)}) collective-permute-start(bf16[128,128]{1,0:T(8,128)(2,1)S(1)} %slice.430), channel_id=1, source_target_pairs={{0,8},{8,16},{16,24},{24,0},{1,9},{9,17},{17,25},{25,1},{2,10},{10... | collective-permute-start | bytes 98312 | tf_op jit(solution)/shard_map/ppermute | solution.py:107
  16.3 4.8 %collective-permute-start = (bf16[3,512]{1,0:T(4,128)(2,1)S(1)}, bf16[3,512]{1,0:T(4,128)(2,1)S(1)}, u32[]{:S(2)}, u32[]{:S(2)}) collective-permute-start(bf16[3,512]{1,0:T(4,128)(2,1)S(1)} %slice.378), channel_id=1, source_target_pairs={{0,8},{8,16},{16,24},{1,9},{9,17},{17,25},{2,10},{10,18},{18,26},{... | collective-permute-start | bytes 9224 | tf_op jit(solution)/shard_map/ppermute | solution.py:16
  50.3 5.8 %collective-permute-start.2 = (bf16[128,128]{1,0:T(8,128)(2,1)S(1)}, bf16[128,128]{1,0:T(8,128)(2,1)S(1)}, u32[]{:S(2)}, u32[]{:S(2)}) collective-permute-start(bf16[128,128]{1,0:T(8,128)(2,1)S(1)} %collective-permute-done.1), channel_id=1, source_target_pairs={{0,8},{8,16},{16,24},{24,0},{1,9},{9,17},{17,25},{25,1},{2,10},{10... | collective-permute-start | bytes 98312 | tf_op jit(solution)/shard_map/ppermute | solution.py:107
  56.1 5.7 %collective-permute-start.3 = (bf16[128,128]{1,0:T(8,128)(2,1)S(1)}, bf16[128,128]{1,0:T(8,128)(2,1)S(1)}, u32[]{:S(2)}, u32[]{:S(2)}) collective-permute-start(bf16[128,128]{1,0:T(8,128)(2,1)S(1)} %collective-permute-done.2), channel_id=1, source_target_pairs={{0,8},{8,16},{16,24},{24,0},{1,9},{9,17},{17,25},{25,1},{2,10},{10... | collective-permute-start | bytes 98312 | tf_op jit(solution)/shard_map/ppermute | solution.py:107
  83.9 6.3 %copy-start.1 = (f32[2048]{0:T(1024)S(1)}, f32[2048]{0:T(1024)}, u32[]{:S(2)}) copy-start(f32[2048]{0:T(1024)} %param.35) | copy-start | bytes 24580
Sparse Core Ops, SparseCore 0:
  8.9 16.3 all-gather.4
  26.8 14.8 all-gather.6
